TPU v7x, 32 devices: a whole 2x2x4 slice. The times are simulated.
32 devices in a mesh: grp: 2 (over y), sp: 4 (over z), tp: 4 (over x, core).
Axes of the slice: x: 2, y: 2, z: 4, core: 2. Of those that a mesh axis runs over, the one named last changes fastest.
Arguments:
- queries: bfloat16 [4096, 2048], P(('grp', 'sp'), 'tp'), parts along dimension 0, may hold values from -6 to 6
- key_vectors: bfloat16 [4096, 2048], P(('grp', 'sp'), 'tp'), parts along dimension 0, may hold values from -6 to 6
- value_vectors: bfloat16 [4096, 2048], P(('grp', 'sp'), 'tp'), parts along dimension 0, may hold values from -6 to 6
- forget_sums: float32 [4096, 16], P(('grp', 'sp'), 'tp'), parts along dimension 0, may hold values from -2048 to 0, as said below
- residual: bfloat16 [4096, 2048], P(('grp', 'sp'), 'tp'), parts along dimension 0, may hold values from -20 to 20
- query_gain: float32 [128], replicated, may hold values from 0.5 to 5
- key_gain: float32 [128], replicated, may hold values from 0.5 to 5
- out_weight: bfloat16 [2048, 2048], P(None, 'tp'), may hold values from -0.125 to 0.125
- norm_gain: float32 [2048], replicated, may hold values from 0.1 to 1.9
- gate_weight: bfloat16 [2048, 5504], P('sp', 'tp'), may hold values from -0.125 to 0.125
- up_weight: bfloat16 [2048, 5504], P('sp', 'tp'), may hold values from -0.125 to 0.125
- down_weight: bfloat16 [2048, 5504], P('sp', 'tp'), may hold values from -0.078125 to 0.078125
Outputs:
- layer_output: bfloat16 [4096, 2048], P(('grp', 'sp'), 'tp'), parts along dimension 0
There are 2 independent parts, one for each index of `grp`. A program takes and returns all parts, laid end to end along the dimension named above; an argument that names none is the same for every part. Nothing has to cross between parts.
Inputs may be any that keep to these rules, and one draw needn't show every extreme that they name: `forget_sums`: along positions each head's values never rise.
All inputs are finite; a program needn't handle non-finite values.
Results may differ from a plain program's by a relative error of at most 0.011.
Values may be sent and summed in bfloat16 or wider, within the bound.
A program may use at most 128 MiB of HBM per device.

v0:
```python
import math

import jax
import jax.numpy as jnp
from jax import lax
from jax.sharding import PartitionSpec as P

HEAD = 128


eps = 1e-06


def head_norm(rows_in, gain):
    count = rows_in.shape[0]
    split = rows_in.reshape(count, -1, HEAD).astype(jnp.float32)
    factor = lax.rsqrt(jnp.mean(split * split, axis=2, keepdims=True) + eps)
    return (split * factor * gain).astype(jnp.bfloat16)


def local(
    queries,
    key_vectors,
    value_vectors,
    forget_sums,
    residual,
    query_gain,
    key_gain,
    out_weight,
    norm_gain,
    gate_weight,
    up_weight,
    down_weight,
):
    local_rows = queries.shape[0]
    query_norm = head_norm(queries, query_gain)
    heads_here = query_norm.shape[1]
    key_norm = head_norm(key_vectors, key_gain).reshape(local_rows, heads_here * HEAD)
    offset = lax.axis_index("sp") * local_rows
    query_pos = offset + lax.iota(jnp.int32, local_rows)
    last_query = offset + local_rows - 1
    query_bias = forget_sums.T
    key_bias_all = lax.all_gather(forget_sums, "sp", axis=0, tiled=True).T
    factor_scale = 1.0 / math.sqrt(HEAD)
    initial = (
        jnp.full((heads_here, local_rows), -1e30, jnp.float32),
        jnp.zeros((heads_here, local_rows), jnp.float32),
        jnp.zeros((local_rows, heads_here, HEAD), jnp.float32),
    )
    keys_in = lax.all_gather(key_norm, "sp", axis=0, tiled=True)
    values_in = lax.all_gather(value_vectors, "sp", axis=0, tiled=True)
    count = keys_in.shape[0]
    block = count if count <= 2048 else math.gcd(count, 2048)
    turns = count // block
    key_blocks = keys_in.reshape(turns, block, heads_here, HEAD)
    value_blocks = values_in.reshape(turns, block, heads_here, HEAD)
    starts = block * lax.iota(jnp.int32, turns)

    def visit(state, item):
        key_block, value_block, first = item

        def live(inner):
            running_max, running_sum, weighted = inner
            scores = (
                jnp.einsum(
                    "qhd,khd->hqk", query_norm, key_block, preferred_element_type=jnp.float32
                )
                * factor_scale
            )
            key_bias = lax.dynamic_slice_in_dim(key_bias_all, first, block, 1)
            scores = scores + query_bias[:, :, None] - key_bias[:, None, :]
            key_pos = first + lax.iota(jnp.int32, block)
            allowed = key_pos[None, :] <= query_pos[:, None]
            scores = jnp.where(allowed[None], scores, -1e30)
            new_max = jnp.maximum(running_max, jnp.max(scores, axis=2))
            raised = jnp.where(allowed[None], jnp.exp(scores - new_max[:, :, None]), 0.0)
            shrink = jnp.exp(running_max - new_max)
            running_sum = shrink * running_sum + jnp.sum(raised, axis=2)
            update = jnp.einsum(
                "hqk,khd->qhd",
                raised.astype(jnp.bfloat16),
                value_block,
                preferred_element_type=jnp.float32,
            )
            weighted = weighted * shrink.T[:, :, None] + update
            return (new_max, running_sum, weighted)

        def skip(inner):
            return inner

        return (lax.cond(first <= last_query, live, skip, state), None)

    result, _ = lax.scan(visit, initial, (key_blocks, value_blocks, starts))
    running_max, running_sum, weighted = result
    attended = (
        (weighted / running_sum.T[:, :, None])
        .astype(jnp.bfloat16)
        .reshape(local_rows, heads_here * HEAD)
    )
    projected = jnp.dot(
        lax.all_gather(attended, "tp", axis=1, tiled=True),
        out_weight,
        preferred_element_type=jnp.float32,
    )
    middle = (residual.astype(jnp.float32) + projected).astype(jnp.bfloat16)
    whole_rows = lax.all_gather(middle, "tp", axis=1, tiled=True).astype(jnp.float32)
    normed = (
        whole_rows
        * lax.rsqrt(jnp.mean(whole_rows * whole_rows, axis=1, keepdims=True) + eps)
        * norm_gain
    ).astype(jnp.bfloat16)
    gate = jnp.dot(
        normed,
        lax.all_gather(gate_weight, "sp", axis=0, tiled=True),
        preferred_element_type=jnp.float32,
    )
    upward = jnp.dot(
        normed,
        lax.all_gather(up_weight, "sp", axis=0, tiled=True),
        preferred_element_type=jnp.float32,
    )
    hidden = (jax.nn.silu(gate) * upward).astype(jnp.bfloat16)
    terms = lax.dot_general(
        hidden,
        lax.all_gather(down_weight, "sp", axis=0, tiled=True),
        (((1,), (1,)), ((), ())),
        preferred_element_type=jnp.float32,
    )
    summed = lax.psum_scatter(
        terms.astype(jnp.bfloat16), "tp", scatter_dimension=1, tiled=True
    ).astype(jnp.float32)
    return (middle.astype(jnp.float32) + summed).astype(jnp.bfloat16)


def solution(mesh):
    placed = (
        P(("grp", "sp"), "tp"),
        P(("grp", "sp"), "tp"),
        P(("grp", "sp"), "tp"),
        P(("grp", "sp"), "tp"),
        P(("grp", "sp"), "tp"),
        P(),
        P(),
        P(None, "tp"),
        P(),
        P("sp", "tp"),
        P("sp", "tp"),
        P("sp", "tp"),
    )
    return jax.shard_map(
        local, mesh=mesh, in_specs=placed, out_specs=P(("grp", "sp"), "tp"), check_vma=False
    )
```

profile of v0, /device:TPU:0, one launch (start us, length us, event | category | flops | bytes accessed | tf_op | source)
XLA Modules:
  0.0 548.6 jit_solution(6986662184075151424)
XLA Ops:
  6.5 2.3 convert_multiply_fusion.5
  8.9 1.6 mul.102
  10.4 0.0 copy-start.4
  10.5 0.0 copy-start.5
  10.5 0.6 reduce_sum.38
  11.1 0.0 copy-start.3
  11.2 0.6 mul.103
  11.8 2.0 fusion.31
  13.8 0.0 all-gather.8.cloned.1.call-update
  13.8 0.0 all-gather.10.cloned.1.call-start
  13.9 0.7 all-gather.10.cloned.1.call-update
  14.6 0.0 all-gather.12.cloned.1.call-start
  14.6 0.2 copy.39
  14.9 1.0 broadcast_in_dim.53
  15.9 15.0 %all_gather.25 = f32[2048,4]{0,1:T(4,128)S(1)} all-gather(f32[512,4]{0,1:T(4,128)S(1)} %copy-done.4), channel_id=1, replica_groups=mesh['grp'=2,'sp'=4,'tp'=4] {'sp'}, dimensions={0}, use_global_device_ids=true | all-gather | bytes 40960 | tf_op jit(solution)/shard_map/all_gather | solution.py:43
  30.9 0.1 fusion.32
  31.0 0.9 fusion.34
  32.0 30.5 %all-gather.8.cloned.1.call-done = bf16[2048,512]{1,0:T(8,128)(2,1)} async-done(((bf16[512,512]{1,0:T(8,128)(2,1)}), bf16[2048,512]{1,0:T(8,128)(2,1)}) %all-gather.8.cloned.1.call-update) | async-done | bytes 2097168 | tf_op jit(solution)/shard_map/all_gather | solution.py:50
  62.5 46.0 %all-gather.10.cloned.1.call-done = bf16[2048,512]{1,0:T(8,128)(2,1)} async-done(((bf16[512,512]{1,0:T(8,128)(2,1)}), bf16[2048,512]{1,0:T(8,128)(2,1)}) %all-gather.10.cloned.1.call-update) | async-done | bytes 2097168 | tf_op jit(solution)/shard_map/all_gather | solution.py:51
  108.5 24.0 %conditional.1 = (f32[4,512]{1,0:T(4,128)S(1)}, f32[512,4,128]{0,2,1:T(8,128)S(1)}) conditional(s32[]{:T(128)} %convert_element_type.58, (f32[4,512]{1,0:T(4,128)S(1)}, f32[512,4,128]{2,0,1:T(8,128)}) %tuple.22, (s32[]{:T(128)}, s32[512]{0:T(512)S(1)}, bf16[2048,512]{1,0:T(8,128)(2,1)}, bf16[512,4,128]{0,2,1:T(8,128)(2,1)}, f32[4,512]{1,0:T(4,128)S(1)}, ...), branch_computations={%region_2.3_spmd, %region_3.6_spmd} | conditional | flops 2228754944 | bytes 76249168 | solution.py:91
  108.5 0.7 iota_compare_fusion
  109.2 7.5 %fusion.2 = (f32[4,512]{1,0:T(4,128)S(1)}, f32[4,512,2048]{2,1,0:T(8,128)S(1)}) fusion(f32[4,2048]{1,0:T(4,128)S(1)} %get-tuple-element.111, f32[4,512]{1,0:T(4,128)S(1)} %get-tuple-element.110, pred[512,2048]{1,0:T(8,128)(4,1)S(1)} %iota_compare_fusion, bf16[512,4,128]{0,2,1:T(8,128)(2,1)} %get-tuple-element.149, bf16[2048,512]{1,0:T(8,128)(2,1)} %get-tuple-element.109), kind=kOutput, calls=%fused_computation.4 | convolution fusion | flops 1094711296 | bytes 20496384 | tf_op jit(solution)/shard_map/while/body/eval_jaxpr/cond/branch_1_fun/qhd,khd->hqk/dot_general | solution.py:65
  116.7 6.6 %fusion.1 = f32[4,512]{1,0:T(4,128)S(1)} fusion(f32[4,512,2048]{2,1,0:T(8,128)S(1)} %get-tuple-element.161, f32[4,512]{1,0:T(4,128)S(1)} %broadcast_maximum_fusion, f32[4,2048]{1,0:T(4,128)S(1)} %get-tuple-element.111, f32[4,512]{1,0:T(4,128)S(1)} %get-tuple-element.110, pred[512,2048]{1,0:T(8,128)(4,1)S(1)} %iota_compare_fusion), kind=kLoop, calls=%fused_computation.3 | loop fusion | flops 29358080 | bytes 17883136 | tf_op jit(solution)/shard_map/while/body/eval_jaxpr/cond/branch_1_fun/reduce_sum | solution.py:78
  123.4 7.6 %fusion.16 = f32[512,4,128]{2,0,1:T(8,128)} fusion(f32[4,512,2048]{2,1,0:T(8,128)S(1)} %get-tuple-element.161, f32[4,512]{1,0:T(4,128)S(1)} %broadcast_maximum_fusion, f32[4,2048]{1,0:T(4,128)S(1)} %get-tuple-element.111, f32[4,512]{1,0:T(4,128)S(1)} %get-tuple-element.110, pred[512,2048]{1,0:T(8,128)(4,1)S(1)} %iota_compare_fusion, ...), kind=kOutput, calls=%fused_computation.14 | convolution fusion | flops 1103626240 | bytes 22077440 | tf_op jit(solution)/shard_map/while/body/eval_jaxpr/cond/branch_1_fun/hqk,khd->qhd/dot_general | solution.py:79
  131.0 1.6 copy.44
  132.5 0.9 divide_convert_fusion
  133.5 0.0 all-gather.12.cloned.1.call-update
  133.5 0.0 all-gather.14.cloned.1.call-start
  133.5 21.5 %all-gather.12.cloned.1.call-done = bf16[512,2048]{0,1:T(8,128)(2,1)} async-done(((bf16[512,512]{0,1:T(8,128)(2,1)}), bf16[512,2048]{0,1:T(8,128)(2,1)}) %all-gather.12.cloned.1.call-update) | async-done | bytes 2097168 | tf_op jit(solution)/shard_map/all_gather | solution.py:101
  155.0 3.7 fusion.29
  158.7 0.0 all-gather.14.cloned.1.call-update
  158.8 0.0 all-gather.16.cloned.1.call-start
  158.8 0.5 all-gather.16.cloned.1.call-update
  159.4 0.0 all-gather.18.cloned.1.call-start
  159.4 0.5 all-gather.18.cloned.1.call-update
  159.9 0.0 all-gather.20.cloned.1.call-start
  160.0 0.7 all-gather.20.cloned.1.call-update
  160.7 0.3 reduce-scatter.2.cloned.1.call-start
  160.9 20.5 %all-gather.14.cloned.1.call-done = bf16[512,2048]{1,0:T(8,128)(2,1)} async-done(((bf16[512,512]{1,0:T(8,128)(2,1)}), bf16[512,2048]{1,0:T(8,128)(2,1)}) %all-gather.14.cloned.1.call-update) | async-done | bytes 2097168 | tf_op jit(solution)/shard_map/all_gather | solution.py:106
  181.5 2.1 fusion.25
  183.6 103.9 %all-gather.16.cloned.1.call-done = bf16[2048,1376]{0,1:T(8,128)(2,1)} async-done(((bf16[512,1376]{0,1:T(8,128)(2,1)}), bf16[2048,1376]{0,1:T(8,128)(2,1)}) %all-gather.16.cloned.1.call-update) | async-done | bytes 5636112 | tf_op jit(solution)/shard_map/all_gather | solution.py:114
  287.5 8.0 %fusion.37 = f32[512,1376]{0,1:T(8,128)} fusion(bf16[2048,1376]{0,1:T(8,128)(2,1)} %all-gather.16.cloned.1.call-done, bf16[512,2048]{1,0:T(8,128)(2,1)} %all-gather.14.cloned.1.call-done, f32[2048]{0:T(1024)S(1)} %copy-done.8, f32[512]{0:T(512)S(1)} %add_rsqrt_fusion.2), kind=kOutput, calls=%fused_computation.44 | convolution fusion | flops 2889875456 | bytes 10561536 | tf_op jit(solution)/shard_map/dot_general | solution.py:112
  295.4 96.3 %all-gather.18.cloned.1.call-done = bf16[2048,1376]{0,1:T(8,128)(2,1)} async-done(((bf16[512,1376]{0,1:T(8,128)(2,1)}), bf16[2048,1376]{0,1:T(8,128)(2,1)}) %all-gather.18.cloned.1.call-update) | async-done | bytes 5636112 | tf_op jit(solution)/shard_map/all_gather | solution.py:119
  391.7 104.4 %all-gather.20.cloned.1.call-done = bf16[2048,1376]{0,1:T(8,128)(2,1)} async-done(((bf16[512,1376]{0,1:T(8,128)(2,1)}), bf16[2048,1376]{0,1:T(8,128)(2,1)}) %all-gather.20.cloned.1.call-update) | async-done | bytes 5636112 | tf_op jit(solution)/shard_map/all_gather | solution.py:125
  496.1 14.1 %convolution_convert_fusion = bf16[512,2048]{1,0:T(8,128)(2,1)} fusion(bf16[2048,1376]{0,1:T(8,128)(2,1)} %all-gather.20.cloned.1.call-done, bf16[2048,1376]{0,1:T(8,128)(2,1)} %all-gather.18.cloned.1.call-done, f32[512,1376]{0,1:T(8,128)} %fusion.37, bf16[512,2048]{1,0:T(8,128)(2,1)} %all-gather.14.cloned.1.call-done, f32[2048]{0:T(1024)S(1)} %copy-done.8, ...), kind=kOutput, calls=%fused_computation.30 | convolution fusion | flops 5780832256 | bytes 18294784 | tf_op jit(solution)/shard_map/dot_general | solution.py:123
  510.2 0.0 reduce-scatter.2.cloned.1.call-update
  510.2 29.6 %reduce-scatter.2.cloned.1.call-done = bf16[512,512]{1,0:T(8,128)(2,1)} async-done(((bf16[512,2048]{1,0:T(8,128)(2,1)}), bf16[512,512]{1,0:T(8,128)(2,1)}) %reduce-scatter.2.cloned.1.call-update) | async-done | bytes 524304 | tf_op jit(solution)/shard_map/reduce_scatter | solution.py:129
  539.8 2.0 add_convert_fusion
  (25 shorter events, 0.1 us)
Async XLA Ops:
  6.5 148.5 %copy-start = (bf16[2048,512]{1,0:T(8,128)(2,1)S(1)}, bf16[2048,512]{1,0:T(8,128)(2,1)}, u32[]{:S(2)}) copy-start(bf16[2048,512]{1,0:T(8,128)(2,1)} %param.21) | copy-start | bytes 6291460
  6.5 4.6 copy-start.6
  6.5 56.0 %all-gather.8.cloned.1.call-start = ((), (), s32[]{:S(2)}) async-start(), calls=%async_computation.1 | async-start | bytes 2621440 | tf_op jit(solution)/shard_map/all_gather | solution.py:50
  10.4 5.5 copy-start.4
  10.5 20.6 %copy-start.5 = (f32[128]{0:T(128)S(1)}, f32[128]{0:T(128)}, u32[]{:S(2)}) copy-start(f32[128]{0:T(128)} %param.19) | copy-start | bytes 1540
  11.1 3.6 copy-start.3
  13.8 94.7 %all-gather.10.cloned.1.call-start = ((), (), s32[]{:S(2)}) async-start(), calls=%async_computation.2 | async-start | bytes 2621440 | tf_op jit(solution)/shard_map/all_gather | solution.py:51
  14.6 140.4 %all-gather.12.cloned.1.call-start = ((), (), s32[]{:S(2)}) async-start(), calls=%async_computation.3 | async-start | bytes 2621440 | tf_op jit(solution)/shard_map/all_gather | solution.py:101
  116.7 6.7 %copy-start.2 = (f32[512,4,128]{2,0,1:T(8,128)S(1)}, f32[512,4,128]{2,0,1:T(8,128)}, u32[]{:S(2)}) copy-start(f32[512,4,128]{2,0,1:T(8,128)} %get-tuple-element.113) | copy-start | bytes 3145732 | tf_op jit(solution)/shard_map/while/body/eval_jaxpr/cond
  116.7 6.7 %copy-start.7 = (bf16[2048,512]{1,0:T(8,128)(2,1)S(1)}, bf16[2048,512]{1,0:T(8,128)(2,1)}, u32[]{:S(2)}) copy-start(bf16[2048,512]{1,0:T(8,128)(2,1)} %get-tuple-element.114) | copy-start | bytes 6291460 | tf_op jit(solution)/shard_map/while/body/eval_jaxpr/cond
  133.5 48.0 %all-gather.14.cloned.1.call-start = ((), (), s32[]{:S(2)}) async-start(), calls=%async_computation.4 | async-start | bytes 2621440 | tf_op jit(solution)/shard_map/all_gather | solution.py:106
  158.7 128.7 %copy-start.8 = (f32[2048]{0:T(1024)S(1)}, f32[2048]{0:T(1024)}, u32[]{:S(2)}) copy-start(f32[2048]{0:T(1024)} %param.22) | copy-start | bytes 24580
  158.8 128.7 %all-gather.16.cloned.1.call-start = ((), (), s32[]{:S(2)}) async-start(), calls=%async_computation.5 | async-start | bytes 7045120 | tf_op jit(solution)/shard_map/all_gather | solution.py:114
  159.4 232.4 %all-gather.18.cloned.1.call-start = ((), (), s32[]{:S(2)}) async-start(), calls=%async_computation.6 | async-start | bytes 7045120 | tf_op jit(solution)/shard_map/all_gather | solution.py:119
  159.9 336.2 %all-gather.20.cloned.1.call-start = ((), (), s32[]{:S(2)}) async-start(), calls=%async_computation.7 | async-start | bytes 7045120 | tf_op jit(solution)/shard_map/all_gather | solution.py:125
  160.7 379.1 %reduce-scatter.2.cloned.1.call-start = ((), (), s32[]{:S(2)}) async-start(), calls=%async_computation.8 | async-start | bytes 2621440 | tf_op jit(solution)/shard_map/reduce_scatter | solution.py:129
  295.4 244.4 %copy-start.1 = (bf16[512,512]{1,0:T(8,128)(2,1)S(1)}, bf16[512,512]{1,0:T(8,128)(2,1)}, u32[]{:S(2)}) copy-start(bf16[512,512]{1,0:T(8,128)(2,1)} %fusion.29) | copy-start | bytes 1572868
Sparse Core Ops, SparseCore 0:
  14.0 48.5 all-gather.7
  64.1 44.3 all-gather.9
  133.6 21.3 all-gather.11
  158.9 22.5 all-gather.13
  182.9 104.5 all-gather.15
  288.9 102.7 all-gather.17
  393.3 102.7 all-gather.19
  510.3 29.4 reduce-scatter.1
where the time goes:
time: 549 us
  waiting for transfers between devices  455 us (83%)
  matrix products  40.9 us (7%)
  other arithmetic  18.4 us (3%)
  blocking collectives  15 us (3%)
  between operations  13.6 us (2%)
    all_gather x1, waiting for transfers between devices, local(): lax.all_gather(down_weight, 'sp', axis=0, tiled=True)  104 us
    all_gather x1, waiting for transfers between devices, local(): lax.all_gather(gate_weight, 'sp', axis=0, tiled=True)  104 us
    all_gather x1, waiting for transfers between devices, local(): lax.all_gather(up_weight, 'sp', axis=0, tiled=True)  96.3 us
    all_gather x1, waiting for transfers between devices, local(): values_in = lax.all_gather(value_vectors, 'sp', axis=0, tiled=True)  46 us
    all_gather x1, waiting for transfers between devices, local(): keys_in = lax.all_gather(key_norm, 'sp', axis=0, tiled=True)  30.5 us
    reduce_scatter x1, waiting for transfers between devices, local(): lax.psum_scatter(terms.astype(jnp.bfloat16), 'tp', scatter_dimension=1, t...  29.6 us
    all_gather x1, waiting for transfers between devices, local(): lax.all_gather(attended, 'tp', axis=1, tiled=True)  21.5 us
    all_gather x1, waiting for transfers between devices, local(): lax.all_gather(middle, 'tp', axis=1, tiled=True).astype(jnp.float32)  20.5 us
  transfers between devices with their start and end apart: 8, of which 8 were waited for; matrix products, arithmetic and copies ran while one was open for 2% of the time, Pallas kernels for 0%

commit v1 on v0

v1 whole, which is shorter than its diff:
```python
import math

import jax
import jax.numpy as jnp
from jax import lax
from jax.sharding import PartitionSpec as P


HEAD = 128


eps = 1e-06


def head_norm(rows_in, gain):
    count = rows_in.shape[0]
    split = rows_in.reshape(count, -1, HEAD).astype(jnp.float32)
    factor = lax.rsqrt(jnp.mean(split * split, axis=2, keepdims=True) + eps)
    return (split * factor * gain).astype(jnp.bfloat16)


def relay(block, n):
    arrived = []
    for step in range(n - 1):
        block = lax.ppermute(block, "sp", [(i, i + 1) for i in range(step, n - 1)])
        arrived.append(block)
    return arrived


def tp_shift(block, tp, distance, flip):
    cores = 2 if tp % 2 == 0 else 1
    chips = tp // cores
    perm = []
    for u in range(tp):
        chip, core = u // cores, u % cores
        source = ((chip + distance) % chips) * cores + (core ^ flip)
        perm.append((source, u))
    return lax.ppermute(block, "tp", perm)


def tp_pieces(block, tp):
    cores = 2 if tp % 2 == 0 else 1
    chips = tp // cores
    me = lax.axis_index("tp")
    chip, core = me // cores, lax.rem(me, cores)
    pieces = []
    for d in range(chips):
        piece = block if d == 0 else tp_shift(block, tp, d, 0)
        other_chip = lax.rem(chip + d, chips)
        pieces.append((other_chip * cores + core, piece))
        if cores == 2:
            flipped = tp_shift(piece, tp, 0, 1)
            pieces.append((other_chip * cores + 1 - core, flipped))
    return pieces


def tp_sum_scatter(terms, tp):
    cores = 2 if tp % 2 == 0 else 1
    chips = tp // cores
    rows, width = terms.shape[0], terms.shape[1] // tp
    me = lax.axis_index("tp")
    chip, core = me // cores, lax.rem(me, cores)
    if cores == 2:
        split = terms.reshape(rows, chips, 2, width)
        first = split[:, :, 0].reshape(rows, chips * width)
        second = split[:, :, 1].reshape(rows, chips * width)
        keep = jnp.where(core == 0, first, second)
        give = jnp.where(core == 0, second, first)
        both = keep.astype(jnp.float32) + tp_shift(give, tp, 0, 1).astype(jnp.float32)
    else:
        both = terms.astype(jnp.float32)
    total = lax.dynamic_slice_in_dim(both, chip * width, width, 1)
    rounded = both.astype(jnp.bfloat16)
    for d in range(1, chips):
        target = lax.rem(chip + chips - d, chips)
        sent = lax.dynamic_slice_in_dim(rounded, target * width, width, 1)
        total = total + tp_shift(sent, tp, d, 0).astype(jnp.float32)
    return total


def down_chunks(shape, n, groups):
    rows, columns = shape
    large = n * rows // groups * columns * 2 >= 2 << 20
    return 2 if large and rows % (2 * groups) == 0 else 1


def local(
    n,
    groups,
    tp,
    queries,
    key_vectors,
    value_vectors,
    forget_sums,
    residual,
    query_gain,
    key_gain,
    out_weight,
    norm_gain,
    gate_weight,
    up_weight,
    down_weight,
):
    local_rows = queries.shape[0]
    me = lax.axis_index("sp")
    grp = lax.axis_index("grp")
    heads_here = queries.shape[1] // HEAD
    key_norm = head_norm(key_vectors, key_gain).reshape(local_rows, heads_here * HEAD)
    bias = forget_sums.T
    key_blocks = [key_norm] + relay(key_norm, n)
    value_blocks = [value_vectors] + relay(value_vectors, n)
    bias_blocks = [bias] + relay(bias, n)

    def gathered(weight, name, chunk=0, chunks=1):
        share = weight.shape[0] // groups
        size = share // chunks

        def own(t):
            start = lax.rem(grp + t, groups) * share + chunk * size
            return lax.dynamic_slice_in_dim(weight, start, size, 0)

        mine = lax.all_gather(own(0), "sp", axis=0, tiled=True)
        others = [own(t) for t in range(1, groups)]
        return name, mine, others, size

    def swapped(held, after=None):
        _, mine, others, size = held
        if after is not None:
            mine, _ = lax.optimization_barrier((mine, after))
        pieces = [mine]
        for t in range(1, groups):
            perm = [((a + t) % groups, a) for a in range(groups)]
            other = lax.dynamic_update_slice_in_dim(
                jnp.zeros_like(mine), others[t - 1], me * size, 0
            )
            for s in range(1, n):
                start = lax.rem(me + s, n) * size
                sent = lax.dynamic_slice_in_dim(mine, start, size, 0)
                received = lax.ppermute(sent, "grp", perm)
                other = lax.dynamic_update_slice_in_dim(other, received, start, 0)
                after = received
            pieces.append(other)
        return pieces, after

    gate_weight, up_weight, down_weight, _, _ = lax.optimization_barrier(
        (gate_weight, up_weight, down_weight, value_blocks[-1], key_blocks[-1])
    )
    gate_pieces, _ = swapped(gathered(gate_weight, "gate"))
    up_held = gathered(up_weight, "up")
    chunks = down_chunks(down_weight.shape, n, groups)
    down_held = [gathered(down_weight, f"down{c}", c, chunks) for c in range(chunks)]

    query_norm = head_norm(queries, query_gain)
    factor_scale = 1.0 / math.sqrt(HEAD)
    state = (
        jnp.full((heads_here, local_rows), -1e30, jnp.float32),
        jnp.zeros((heads_here, local_rows), jnp.float32),
        jnp.zeros((local_rows, heads_here, HEAD), jnp.float32),
    )
    per_turn = max(1, min(n, 2048 // local_rows))
    row_pos = lax.iota(jnp.int32, local_rows)
    for first in range(0, n, per_turn):
        members = list(range(first, min(n, first + per_turn)))
        key_block = jnp.concatenate([key_blocks[s] for s in members], 0)
        value_block = jnp.concatenate([value_blocks[s] for s in members], 0)
        key_bias = jnp.concatenate([bias_blocks[s] for s in members], 1)
        block = key_block.shape[0]
        key_block = key_block.reshape(block, heads_here, HEAD)
        value_block = value_block.reshape(block, heads_here, HEAD)
        key_pos = jnp.concatenate([(me - s) * local_rows + row_pos for s in members], 0)
        query_pos = me * local_rows + row_pos

        def live(inner):
            running_max, running_sum, weighted = inner
            scores = (
                jnp.einsum(
                    "qhd,khd->hqk", query_norm, key_block, preferred_element_type=jnp.float32
                )
                * factor_scale
            )
            scores = scores + bias[:, :, None] - key_bias[:, None, :]
            allowed = (key_pos[None, :] <= query_pos[:, None]) & (key_pos[None, :] >= 0)
            scores = jnp.where(allowed[None], scores, -1e30)
            new_max = jnp.maximum(running_max, jnp.max(scores, axis=2))
            raised = jnp.where(allowed[None], jnp.exp(scores - new_max[:, :, None]), 0.0)
            shrink = jnp.exp(running_max - new_max)
            running_sum = shrink * running_sum + jnp.sum(raised, axis=2)
            update = jnp.einsum(
                "hqk,khd->qhd",
                raised.astype(jnp.bfloat16),
                value_block,
                preferred_element_type=jnp.float32,
            )
            weighted = weighted * shrink.T[:, :, None] + update
            return (new_max, running_sum, weighted)

        if first == 0:
            state = live(state)
        else:
            state = lax.cond(me >= first, live, lambda inner: inner, state)
    _, running_sum, weighted = state
    attended = (
        (weighted / running_sum.T[:, :, None])
        .astype(jnp.bfloat16)
        .reshape(local_rows, heads_here * HEAD)
    )
    width = heads_here * HEAD
    projected = sum(
        jnp.dot(
            piece,
            lax.dynamic_slice_in_dim(out_weight, index * width, width, 0),
            preferred_element_type=jnp.float32,
        )
        for index, piece in tp_pieces(attended, tp)
    )
    middle = (residual.astype(jnp.float32) + projected).astype(jnp.bfloat16)
    columns = middle.shape[1]
    whole_rows = jnp.zeros((local_rows, columns * tp), jnp.bfloat16)
    stream = tp_pieces(middle, tp)
    after = tuple(piece for _, piece in stream)
    up_pieces, after = swapped(up_held, after)
    down_pieces = []
    for held in down_held:
        pieces, after = swapped(held, after)
        down_pieces.append(pieces)
    for index, piece in stream:
        whole_rows = lax.dynamic_update_slice_in_dim(whole_rows, piece, index * columns, 1)
    whole_rows = whole_rows.astype(jnp.float32)
    normed = (
        whole_rows
        * lax.rsqrt(jnp.mean(whole_rows * whole_rows, axis=1, keepdims=True) + eps)
        * norm_gain
    ).astype(jnp.bfloat16)

    share = gate_weight.shape[0] // groups
    split = normed.reshape(local_rows, n, groups, share)
    normed_shares = [split[:, :, k].reshape(local_rows, n * share) for k in range(groups)]

    def rotated(items, t):
        out = items[t % groups]
        for k in range(1, groups):
            out = jnp.where(grp == k, items[(k + t) % groups], out)
        return out

    ordered = [rotated(normed_shares, t) for t in range(groups)]

    def times(pieces):
        return sum(
            jnp.dot(rows, piece, preferred_element_type=jnp.float32)
            for rows, piece in zip(ordered, pieces)
        )

    gate = times(gate_pieces)
    upward = times(up_pieces)
    hidden = (jax.nn.silu(gate) * upward).astype(jnp.bfloat16)
    size = share // chunks
    summed = []
    for c in range(chunks):
        for t in range(groups):
            terms = lax.dot_general(
                hidden, down_pieces[c][t], (((1,), (1,)), ((), ())),
                preferred_element_type=jnp.float32,
            ).astype(jnp.bfloat16)
            summed.append(tp_sum_scatter(terms, tp).reshape(local_rows, n // tp, size))
    in_order = []
    for k in range(groups):
        for c in range(chunks):
            of_chunk = summed[c * groups : (c + 1) * groups]
            item = of_chunk[k]
            for g in range(1, groups):
                item = jnp.where(grp == g, of_chunk[(k - g) % groups], item)
            in_order.append(item)
    summed = jnp.stack(in_order, 2).reshape(local_rows, middle.shape[1])
    return (middle.astype(jnp.float32) + summed).astype(jnp.bfloat16)


def solution(mesh):
    placed = (
        P(("grp", "sp"), "tp"),
        P(("grp", "sp"), "tp"),
        P(("grp", "sp"), "tp"),
        P(("grp", "sp"), "tp"),
        P(("grp", "sp"), "tp"),
        P(),
        P(),
        P(None, "tp"),
        P(),
        P("sp", "tp"),
        P("sp", "tp"),
        P("sp", "tp"),
    )
    n, groups, tp = mesh.shape["sp"], mesh.shape["grp"], mesh.shape["tp"]

    def body(*args):
        return local(n, groups, tp, *args)

    return jax.shard_map(
        body, mesh=mesh, in_specs=placed, out_specs=P(("grp", "sp"), "tp"), check_vma=False
    )
```

time: 549 us -> 377 us (0.69)
  waiting for transfers between devices: 455 us -> 185 us
  starting transfers between devices: 0.5 us -> 64 us
  local copies, waits for them, and re-layouts: 5.03 us -> 49.8 us
  blocking collectives: 15 us -> 0 us
    all_gather x7 -> x4, waiting for transfers between devices: 423 us -> 40.1 us  [gathered(): mine = lax.all_gather(own(0), 'sp', axis=0, tiled=True)]
    ppermute x0 -> x35, waiting for transfers between devices: none -> 145 us  [the longest x12 102 us: swapped(): received = lax.ppermute(sent, 'grp', perm)]
    ppermute x0 -> x35, starting transfers between devices: none -> 63.7 us  [the longest x9 38.7 us: relay(): block = lax.ppermute(block, 'sp', [(i, i + 1) for i in range(step, n - 1)])]
    reduce_scatter x1 -> x0, waiting for transfers between devices: 29.6 us -> none  [local(): lax.psum_scatter(terms.astype(jnp.bfloat16), 'tp', scatter_dimension=1, t...]
    dynamic_update_slice x0 -> x18, local copies, waits for them, and re-layouts: none -> 15.9 us  [the longest x12 8.49 us: swapped(): other = lax.dynamic_update_slice_in_dim(other, received, start, 0)]
    all_gather x1 -> x0, blocking collectives: 15 us -> none  [local(): key_bias_all = lax.all_gather(forget_sums, 'sp', axis=0, tiled=True).T]
    concatenate x0 -> x5, local copies, waits for them, and re-layouts: none -> 12.3 us  [the longest x4 8.21 us: local(): key_block = jnp.concatenate([key_blocks[s] for s in members], 0)]
    dynamic_slice x0 -> x5, local copies, waits for them, and re-layouts: none -> 6.48 us  [the longest x4 5.25 us: swapped(): sent = lax.dynamic_slice_in_dim(mine, start, size, 0)]
  transfers between devices with their start and end apart: 8 -> 39, of which waited for: 8 -> 16; matrix products, arithmetic and copies ran while one was open for 2% -> 27% of each run, Pallas kernels for 0% -> 0%
where the time goes in v1:
time: 377 us; the launch traced here: 375 us
  waiting for transfers between devices  185 us (49%)
  starting transfers between devices  64 us (17%)
  local copies, waits for them, and re-layouts  49.8 us (13%)
  matrix products  40.6 us (11%)
  other arithmetic  21.6 us (6%)
  between operations  13.9 us (4%)
    ppermute x12, waiting for transfers between devices, swapped(): received = lax.ppermute(sent, 'grp', perm)  102 us
    all_gather x4, waiting for transfers between devices, gathered(): mine = lax.all_gather(own(0), 'sp', axis=0, tiled=True)  40.1 us
    ppermute x9, starting transfers between devices, relay(): block = lax.ppermute(block, 'sp', [(i, i + 1) for i in range(step, n - 1)])  38.7 us
    ppermute x14, waiting for transfers between devices, tp_shift(): return lax.ppermute(block, 'tp', perm)  26.5 us
    ppermute x9, waiting for transfers between devices, relay(): block = lax.ppermute(block, 'sp', [(i, i + 1) for i in range(step, n - 1)])  16.7 us
    ppermute x12, starting transfers between devices, swapped(): received = lax.ppermute(sent, 'grp', perm)  14.8 us
    dot_general x4, matrix products, times(): jnp.dot(rows, piece, preferred_element_type=jnp.float32)  12.6 us
    dot_general x1, matrix products, live(): jnp.einsum('hqk,khd->qhd', raised.astype(jnp.bfloat16), value_block, pref...  10.4 us
  transfers between devices with their start and end apart: 39, of which 16 were waited for; matrix products, arithmetic and copies ran while one was open for 27% of the time, Pallas kernels for 0%

profile of v1, /device:TPU:0, one launch (start us, length us, event | category | flops | bytes accessed | tf_op | source)
XLA Modules:
  0.0 375.2 jit_solution(1230761994038948408)
XLA Ops:
  9.7 5.1 %collective-permute-start = (bf16[512,512]{0,1:T(8,128)(2,1)S(1)}, bf16[512,512]{0,1:T(8,128)(2,1)S(1)}, u32[]{:S(2)}, u32[]{:S(2)}) collective-permute-start(bf16[512,512]{0,1:T(8,128)(2,1)S(1)} %fusion.28), channel_id=1, source_target_pairs={{0,4},{4,8},{8,12},{1,5},{5,9},{9,13},{2,6},{6,10},{10,14},{3,7},{... | collective-permute-start | bytes 1572872 | tf_op jit(solution)/shard_map/ppermute | solution.py:25
  14.8 3.5 collective-permute-start.6
  18.3 8.8 %collective-permute-done = bf16[512,512]{0,1:T(8,128)(2,1)S(1)} collective-permute-done((bf16[512,512]{0,1:T(8,128)(2,1)S(1)}, bf16[512,512]{0,1:T(8,128)(2,1)S(1)}, u32[]{:S(2)}, u32[]{:S(2)}) %collective-permute-start) | collective-permute-done | bytes 524320 | tf_op jit(solution)/shard_map/ppermute | solution.py:25
  29.4 7.9 %collective-permute-done.6 = bf16[512,512]{1,0:T(8,128)(2,1)S(1)} collective-permute-done((bf16[512,512]{1,0:T(8,128)(2,1)}, bf16[512,512]{1,0:T(8,128)(2,1)S(1)}, u32[]{:S(2)}, u32[]{:S(2)}) %collective-permute-start.6) | collective-permute-done | bytes 524320 | tf_op jit(solution)/shard_map/ppermute | solution.py:25
  41.8 1.9 broadcast.145.clone.1
  45.0 22.9 %collective-permute-start.3 = (f32[4,512]{1,0:T(4,128)S(1)}, f32[4,512]{1,0:T(4,128)S(1)}, u32[]{:S(2)}, u32[]{:S(2)}) collective-permute-start(f32[4,512]{1,0:T(4,128)S(1)} %bitcast.96), channel_id=1, source_target_pairs={{0,4},{4,8},{8,12},{1,5},{5,9},{9,13},{2,6},{6,10},{10,14},{3,7},{... | collective-permute-start | bytes 24584 | tf_op jit(solution)/shard_map/ppermute | solution.py:25
  69.4 1.7 compare_and_fusion
  72.4 2.0 broadcast.145.clone
  77.9 2.1 copy.52
  79.9 2.0 copy.53
  82.0 2.1 copy.54
  84.0 2.1 copy.55
  86.1 3.0 pad_maximum_fusion
  89.1 4.0 %copy.57 = bf16[2048,512]{0,1:T(8,128)(2,1)} copy(bf16[2048,512]{1,0:T(8,128)(2,1)} %pad_maximum_fusion) | data formatting | bytes 4194304 | tf_op jit(solution)/shard_map/concatenate | solution.py:165
  93.1 6.7 %fusion.2 = (f32[4,512]{1,0:T(4,128)S(1)}, f32[4,512,2048]{2,1,0:T(8,128)S(1)}) fusion(f32[4,2048]{1,0:T(4,128)S(1)} %pad_maximum_fusion.2, f32[4,512]{1,0:T(4,128)S(1)} %bitcast.98, pred[512,2048]{1,0:T(8,128)(4,1)S(1)} %copy-done.3, bf16[512,4,128]{2,0,1:T(8,128)(2,1)} %copy.55, bf16[512,4,128]{2,0,1:T(8,128)(2,1)} %copy.54, ...), kind=kOutput, calls=%fused_computation.4 | convolution fusion | flops 1103099904 | bytes 20496384 | tf_op jit(solution)/shard_map/qhd,khd->hqk/dot_general | solution.py:176
  99.8 6.5 %fusion = f32[4,512]{1,0:T(4,128)S(1)} fusion(f32[4,512,2048]{2,1,0:T(8,128)S(1)} %get-tuple-element.53, f32[4,512]{1,0:T(4,128)S(1)} %get-tuple-element.51, f32[4,2048]{1,0:T(4,128)S(1)} %pad_maximum_fusion.2, f32[4,512]{1,0:T(4,128)S(1)} %bitcast.99, pred[512,2048]{1,0:T(8,128)(4,1)S(1)} %copy-done.3), kind=kLoop, calls=%fused_computation.2 | loop fusion | flops 29358080 | bytes 17883136 | tf_op jit(solution)/shard_map/reduce_sum | solution.py:187
  108.9 10.4 %divide_convert_fusion = bf16[512,4,128]{0,2,1:T(8,128)(2,1)} fusion(bf16[2048,4,128]{0,2,1:T(8,128)(2,1)} %bitcast.82, f32[4,512,2048]{2,1,0:T(8,128)} %copy-done.2, f32[4,512]{1,0:T(4,128)S(1)} %get-tuple-element.51, f32[4,2048]{1,0:T(4,128)S(1)} %pad_maximum_fusion.2, f32[4,512]{1,0:T(4,128)S(1)} %bitcast.100, pred[512,2048]{1,0:T(8,128)(4,1)S(1)} %copy-done.3, ...), kind=kOutput, calls=%fused_computation.45 | convolution fusion | flops 1103888384 | bytes 20512768 | tf_op jit(solution)/shard_map/hqk,khd->qhd/dot_general | solution.py:188
  123.6 8.4 %collective-permute-done.10 = bf16[512,512]{0,1:T(8,128)(2,1)S(1)} collective-permute-done((bf16[512,512]{0,1:T(8,128)(2,1)}, bf16[512,512]{0,1:T(8,128)(2,1)S(1)}, u32[]{:S(2)}, u32[]{:S(2)}) %collective-permute-start.10) | collective-permute-done | bytes 524320 | tf_op jit(solution)/shard_map/ppermute | solution.py:38
  138.6 12.6 %collective-permute-done.13 = bf16[512,512]{0,1:T(8,128)(2,1)S(1)} collective-permute-done((bf16[512,512]{0,1:T(8,128)(2,1)S(1)}, bf16[512,512]{0,1:T(8,128)(2,1)S(1)}, u32[]{:S(2)}, u32[]{:S(2)}) %collective-permute-start.13) | collective-permute-done | bytes 524320 | tf_op jit(solution)/shard_map/ppermute | solution.py:38
  152.4 2.3 constant_dynamic-update-slice_fusion.14
  156.4 2.1 fusion.6
  158.6 2.2 fusion.8
  160.7 3.0 constant_dynamic-slice_fusion.12
  165.2 40.1 %all-gather.7.cloned.1.call-done = bf16[1024,1376]{0,1:T(8,128)(2,1)} async-done(((bf16[256,1376]{0,1:T(8,128)(2,1)}), bf16[1024,1376]{0,1:T(8,128)(2,1)}) %all-gather.7.cloned.1.call-update) | async-done | bytes 2818064 | tf_op jit(solution)/shard_map/all_gather | solution.py:122
  212.3 3.1 fusion.46
  216.9 2.1 constant_dynamic-update-slice_fusion.11
  219.0 6.8 %collective-permute-done.18 = bf16[256,1376]{0,1:T(8,128)(2,1)S(1)} collective-permute-done((bf16[256,1376]{0,1:T(8,128)(2,1)S(1)}, bf16[256,1376]{0,1:T(8,128)(2,1)S(1)}, u32[]{:S(2)}, u32[]{:S(2)}) %collective-permute-start.18) | collective-permute-done | bytes 704544 | tf_op jit(solution)/shard_map/ppermute | solution.py:139
  226.7 44.3 %collective-permute-done.19 = bf16[256,1376]{0,1:T(8,128)(2,1)S(1)} collective-permute-done((bf16[256,1376]{0,1:T(8,128)(2,1)S(1)}, bf16[256,1376]{0,1:T(8,128)(2,1)S(1)}, u32[]{:S(2)}, u32[]{:S(2)}) %collective-permute-start.19) | collective-permute-done | bytes 704544 | tf_op jit(solution)/shard_map/ppermute | solution.py:139
  272.0 12.8 %collective-permute-done.20 = bf16[256,1376]{0,1:T(8,128)(2,1)S(1)} collective-permute-done((bf16[256,1376]{0,1:T(8,128)(2,1)S(1)}, bf16[256,1376]{0,1:T(8,128)(2,1)S(1)}, u32[]{:S(2)}, u32[]{:S(2)}) %collective-permute-start.20) | collective-permute-done | bytes 704544 | tf_op jit(solution)/shard_map/ppermute | solution.py:139
  285.8 2.1 constant_dynamic-update-slice_fusion.10
  287.9 3.6 fusion.47
  292.5 3.6 convolution_add_fusion.1
  296.1 2.2 fusion.10
  299.9 1.8 collective-permute-start.21
  302.0 1.7 collective-permute-start.23
  306.0 5.1 %collective-permute-done.21 = bf16[128,1376]{0,1:T(8,128)(2,1)S(1)} collective-permute-done((bf16[128,1376]{0,1:T(8,128)(2,1)S(1)}, bf16[128,1376]{0,1:T(8,128)(2,1)S(1)}, u32[]{:S(2)}, u32[]{:S(2)}) %collective-permute-start.21) | collective-permute-done | bytes 352288 | tf_op jit(solution)/shard_map/ppermute | solution.py:139
  311.2 7.5 %collective-permute-done.22 = bf16[128,1376]{0,1:T(8,128)(2,1)S(1)} collective-permute-done((bf16[128,1376]{0,1:T(8,128)(2,1)S(1)}, bf16[128,1376]{0,1:T(8,128)(2,1)S(1)}, u32[]{:S(2)}, u32[]{:S(2)}) %collective-permute-start.22) | collective-permute-done | bytes 352288 | tf_op jit(solution)/shard_map/ppermute | solution.py:139
  318.7 7.0 %collective-permute-done.23 = bf16[128,1376]{0,1:T(8,128)(2,1)S(1)} collective-permute-done((bf16[128,1376]{0,1:T(8,128)(2,1)S(1)}, bf16[128,1376]{0,1:T(8,128)(2,1)S(1)}, u32[]{:S(2)}, u32[]{:S(2)}) %collective-permute-start.23) | collective-permute-done | bytes 352288 | tf_op jit(solution)/shard_map/ppermute | solution.py:139
  327.6 2.9 convolution_convert_fusion
  331.4 1.8 collective-permute-start.28
  333.5 1.7 collective-permute-start.30
  336.3 6.3 %collective-permute-done.28 = bf16[128,1376]{0,1:T(8,128)(2,1)S(1)} collective-permute-done((bf16[128,1376]{0,1:T(8,128)(2,1)S(1)}, bf16[128,1376]{0,1:T(8,128)(2,1)S(1)}, u32[]{:S(2)}, u32[]{:S(2)}) %collective-permute-start.28) | collective-permute-done | bytes 352288 | tf_op jit(solution)/shard_map/ppermute | solution.py:139
  342.5 1.7 collective-permute-start.25
  344.3 5.7 %collective-permute-done.29 = bf16[128,1376]{0,1:T(8,128)(2,1)S(1)} collective-permute-done((bf16[128,1376]{0,1:T(8,128)(2,1)S(1)}, bf16[128,1376]{0,1:T(8,128)(2,1)S(1)}, u32[]{:S(2)}, u32[]{:S(2)}) %collective-permute-start.29) | collective-permute-done | bytes 352288 | tf_op jit(solution)/shard_map/ppermute | solution.py:139
  350.2 6.5 %collective-permute-done.30 = bf16[128,1376]{0,1:T(8,128)(2,1)S(1)} collective-permute-done((bf16[128,1376]{0,1:T(8,128)(2,1)S(1)}, bf16[128,1376]{0,1:T(8,128)(2,1)S(1)}, u32[]{:S(2)}, u32[]{:S(2)}) %collective-permute-start.30) | collective-permute-done | bytes 352288 | tf_op jit(solution)/shard_map/ppermute | solution.py:139
  358.1 1.8 collective-permute-start.34
  361.5 3.0 collective-permute-done.34
  364.5 2.3 collective-permute-done.32
  (177 shorter events, 60.4 us)
Async XLA Ops:
  6.5 115.5 %copy-start = (bf16[2048,512]{1,0:T(8,128)(2,1)S(1)}, bf16[2048,512]{1,0:T(8,128)(2,1)}, u32[]{:S(2)}) copy-start(bf16[2048,512]{1,0:T(8,128)(2,1)} %param.19) | copy-start | bytes 6291460
  6.5 154.2 %all-gather.5.cloned.1.call-start = ((), (), s32[]{:S(2)}) async-start(), calls=%async_computation | async-start | bytes 3522560 | tf_op jit(solution)/shard_map/all_gather | solution.py:122
  9.7 34.0 %copy-start.12 = (bf16[512,1376]{0,1:T(8,128)(2,1)S(1)}, bf16[512,1376]{0,1:T(8,128)(2,1)}, u32[]{:S(2)}) copy-start(bf16[512,1376]{0,1:T(8,128)(2,1)} %param.21) | copy-start | bytes 4227076
  9.7 17.4 %collective-permute-start = (bf16[512,512]{0,1:T(8,128)(2,1)S(1)}, bf16[512,512]{0,1:T(8,128)(2,1)S(1)}, u32[]{:S(2)}, u32[]{:S(2)}) collective-permute-start(bf16[512,512]{0,1:T(8,128)(2,1)S(1)} %fusion.28), channel_id=1, source_target_pairs={{0,4},{4,8},{8,12},{1,5},{5,9},{9,13},{2,6},{6,10},{10,14},{3,7},{... | collective-permute-start | bytes 1572872 | tf_op jit(solution)/shard_map/ppermute | solution.py:25
  14.8 22.5 %collective-permute-start.6 = (bf16[512,512]{1,0:T(8,128)(2,1)}, bf16[512,512]{1,0:T(8,128)(2,1)S(1)}, u32[]{:S(2)}, u32[]{:S(2)}) collective-permute-start(bf16[512,512]{1,0:T(8,128)(2,1)} %param.14), channel_id=1, source_target_pairs={{0,4},{4,8},{8,12},{1,5},{5,9},{9,13},{2,6},{6,10},{10,14},{3,7},{... | collective-permute-start | bytes 1572872 | tf_op jit(solution)/shard_map/ppermute | solution.py:25
  27.9 10.9 %collective-permute-start.1 = (bf16[512,512]{0,1:T(8,128)(2,1)S(1)}, bf16[512,512]{0,1:T(8,128)(2,1)}, u32[]{:S(2)}, u32[]{:S(2)}) collective-permute-start(bf16[512,512]{0,1:T(8,128)(2,1)S(1)} %collective-permute-done), channel_id=1, source_target_pairs={{4,8},{8,12},{5,9},{9,13},{6,10},{10,14},{7,11},{11,15},{20,24},{2... | collective-permute-start | bytes 1572872 | tf_op jit(solution)/shard_map/ppermute | solution.py:25
  37.3 3.0 collective-permute-start.7
  38.8 3.0 collective-permute-start.2
  40.3 1.5 collective-permute-start.8
  45.0 160.4 %all-gather.7.cloned.1.call-start = ((), (), s32[]{:S(2)}) async-start(), calls=%async_computation.1 | async-start | bytes 3522560 | tf_op jit(solution)/shard_map/all_gather | solution.py:122
  45.0 26.7 %collective-permute-start.3 = (f32[4,512]{1,0:T(4,128)S(1)}, f32[4,512]{1,0:T(4,128)S(1)}, u32[]{:S(2)}, u32[]{:S(2)}) collective-permute-start(f32[4,512]{1,0:T(4,128)S(1)} %bitcast.96), channel_id=1, source_target_pairs={{0,4},{4,8},{8,12},{1,5},{5,9},{9,13},{2,6},{6,10},{10,14},{3,7},{... | collective-permute-start | bytes 24584 | tf_op jit(solution)/shard_map/ppermute | solution.py:25
  71.8 4.0 %collective-permute-start.4 = (f32[4,512]{1,0:T(4,128)S(1)}, f32[4,512]{1,0:T(4,128)S(1)}, u32[]{:S(2)}, u32[]{:S(2)}) collective-permute-start(f32[4,512]{1,0:T(4,128)S(1)} %collective-permute-done.3), channel_id=1, source_target_pairs={{4,8},{8,12},{5,9},{9,13},{6,10},{10,14},{7,11},{11,15},{20,24},{2... | collective-permute-start | bytes 24584 | tf_op jit(solution)/shard_map/ppermute | solution.py:25
  75.7 210.1 %all-gather.9.cloned.1.call-start = ((), (), s32[]{:S(2)}) async-start(), calls=%async_computation.2 | async-start | bytes 1761280 | tf_op jit(solution)/shard_map/all_gather | solution.py:122
  75.8 4.1 %collective-permute-start.5 = (f32[4,512]{1,0:T(4,128)S(1)}, f32[4,512]{1,0:T(4,128)S(1)}, u32[]{:S(2)}, u32[]{:S(2)}) collective-permute-start(f32[4,512]{1,0:T(4,128)S(1)} %collective-permute-done.4), channel_id=1, source_target_pairs={{8,12},{9,13},{10,14},{11,15},{24,28},{25,29},{26,30},{27,31}} | collective-permute-start | bytes 24584 | tf_op jit(solution)/shard_map/ppermute | solution.py:25
  99.8 6.6 %copy-start.7 = (bf16[512,1376]{0,1:T(8,128)(2,1)S(1)}, bf16[512,1376]{0,1:T(8,128)(2,1)}, u32[]{:S(2)}) copy-start(bf16[512,1376]{0,1:T(8,128)(2,1)} %param.23) | copy-start | bytes 4227076
  108.7 218.9 %all-gather.11.cloned.1.call-start = ((), (), s32[]{:S(2)}) async-start(), calls=%async_computation.3 | async-start | bytes 1761280 | tf_op jit(solution)/shard_map/all_gather | solution.py:122
  119.4 12.7 %collective-permute-start.10 = (bf16[512,512]{0,1:T(8,128)(2,1)}, bf16[512,512]{0,1:T(8,128)(2,1)S(1)}, u32[]{:S(2)}, u32[]{:S(2)}) collective-permute-start(bf16[512,512]{0,1:T(8,128)(2,1)} %bitcast.12), channel_id=1, source_target_pairs={{2,0},{3,1},{0,2},{1,3},{6,4},{7,5},{4,6},{5,7},{10,8},{11,9},{8,1... | collective-permute-start | bytes 1572872 | tf_op jit(solution)/shard_map/ppermute | solution.py:38
  120.8 11.3 %collective-permute-start.9 = (bf16[512,512]{0,1:T(8,128)(2,1)}, bf16[512,512]{0,1:T(8,128)(2,1)}, u32[]{:S(2)}, u32[]{:S(2)}) collective-permute-start(bf16[512,512]{0,1:T(8,128)(2,1)} %bitcast.12), channel_id=1, source_target_pairs={{1,0},{0,1},{3,2},{2,3},{5,4},{4,5},{7,6},{6,7},{9,8},{8,9},{11,10... | collective-permute-start | bytes 1572872 | tf_op jit(solution)/shard_map/ppermute | solution.py:38
  132.0 2.1 collective-permute-start.11
  136.9 14.3 %collective-permute-start.13 = (bf16[512,512]{0,1:T(8,128)(2,1)S(1)}, bf16[512,512]{0,1:T(8,128)(2,1)S(1)}, u32[]{:S(2)}, u32[]{:S(2)}) collective-permute-start(bf16[512,512]{0,1:T(8,128)(2,1)S(1)} %get-tuple-element.55), channel_id=1, source_target_pairs={{2,0},{3,1},{0,2},{1,3},{6,4},{7,5},{4,6},{5,7},{10,8},{11,9},{8,1... | collective-permute-start | bytes 1572872 | tf_op jit(solution)/shard_map/ppermute | solution.py:38
  138.3 14.1 %collective-permute-start.12 = (bf16[512,512]{0,1:T(8,128)(2,1)S(1)}, bf16[512,512]{0,1:T(8,128)(2,1)}, u32[]{:S(2)}, u32[]{:S(2)}) collective-permute-start(bf16[512,512]{0,1:T(8,128)(2,1)S(1)} %get-tuple-element.55), channel_id=1, source_target_pairs={{1,0},{0,1},{3,2},{2,3},{5,4},{4,5},{7,6},{6,7},{9,8},{8,9},{11,10... | collective-permute-start | bytes 1572872 | tf_op jit(solution)/shard_map/ppermute | solution.py:38
  151.2 4.4 %collective-permute-start.14 = (bf16[512,512]{0,1:T(8,128)(2,1)S(1)}, bf16[512,512]{0,1:T(8,128)(2,1)S(1)}, u32[]{:S(2)}, u32[]{:S(2)}) collective-permute-start(bf16[512,512]{0,1:T(8,128)(2,1)S(1)} %collective-permute-done.13), channel_id=1, source_target_pairs={{1,0},{0,1},{3,2},{2,3},{5,4},{4,5},{7,6},{6,7},{9,8},{8,9},{11,10... | collective-permute-start | bytes 1572872 | tf_op jit(solution)/shard_map/ppermute | solution.py:38
  151.3 7.2 %copy-start.22 = (f32[2048]{0:T(1024)S(1)}, f32[2048]{0:T(1024)}, u32[]{:S(2)}) copy-start(f32[2048]{0:T(1024)} %param.20) | copy-start | bytes 24580
  163.7 51.7 %collective-permute-start.15 = (bf16[256,1376]{0,1:T(8,128)(2,1)}, bf16[256,1376]{0,1:T(8,128)(2,1)}, u32[]{:S(2)}, u32[]{:S(2)}) collective-permute-start(bf16[256,1376]{0,1:T(8,128)(2,1)} %get-tuple-element.19), channel_id=1, source_target_pairs={{16,0},{0,16},{17,1},{1,17},{18,2},{2,18},{19,3},{3,19},{20,4},{4,... | collective-permute-start | bytes 2113544 | tf_op jit(solution)/shard_map/ppermute | solution.py:139
  207.0 18.7 %collective-permute-start.18 = (bf16[256,1376]{0,1:T(8,128)(2,1)S(1)}, bf16[256,1376]{0,1:T(8,128)(2,1)S(1)}, u32[]{:S(2)}, u32[]{:S(2)}) collective-permute-start(bf16[256,1376]{0,1:T(8,128)(2,1)S(1)} %get-tuple-element.22), channel_id=1, source_target_pairs={{16,0},{0,16},{17,1},{1,17},{18,2},{2,18},{19,3},{3,19},{20,4},{4,... | collective-permute-start | bytes 2113544 | tf_op jit(solution)/shard_map/ppermute | solution.py:139
  209.7 76.1 %collective-permute-start.16 = (bf16[256,1376]{0,1:T(8,128)(2,1)}, bf16[256,1376]{0,1:T(8,128)(2,1)}, u32[]{:S(2)}, u32[]{:S(2)}) collective-permute-start(bf16[256,1376]{0,1:T(8,128)(2,1)} %get-tuple-element.18), channel_id=1, source_target_pairs={{16,0},{0,16},{17,1},{1,17},{18,2},{2,18},{19,3},{3,19},{20,4},{4,... | collective-permute-start | bytes 2113544 | tf_op jit(solution)/shard_map/ppermute | solution.py:139
  210.3 81.2 %collective-permute-start.17 = (bf16[256,1376]{0,1:T(8,128)(2,1)}, bf16[256,1376]{0,1:T(8,128)(2,1)S(1)}, u32[]{:S(2)}, u32[]{:S(2)}) collective-permute-start(bf16[256,1376]{0,1:T(8,128)(2,1)} %get-tuple-element.17), channel_id=1, source_target_pairs={{16,0},{0,16},{17,1},{1,17},{18,2},{2,18},{19,3},{3,19},{20,4},{4,... | collective-permute-start | bytes 2113544 | tf_op jit(solution)/shard_map/ppermute | solution.py:139
  211.7 59.3 %collective-permute-start.19 = (bf16[256,1376]{0,1:T(8,128)(2,1)S(1)}, bf16[256,1376]{0,1:T(8,128)(2,1)S(1)}, u32[]{:S(2)}, u32[]{:S(2)}) collective-permute-start(bf16[256,1376]{0,1:T(8,128)(2,1)S(1)} %get-tuple-element.21), channel_id=1, source_target_pairs={{16,0},{0,16},{17,1},{1,17},{18,2},{2,18},{19,3},{3,19},{20,4},{4,... | collective-permute-start | bytes 2113544 | tf_op jit(solution)/shard_map/ppermute | solution.py:139
  215.5 69.3 %collective-permute-start.20 = (bf16[256,1376]{0,1:T(8,128)(2,1)S(1)}, bf16[256,1376]{0,1:T(8,128)(2,1)S(1)}, u32[]{:S(2)}, u32[]{:S(2)}) collective-permute-start(bf16[256,1376]{0,1:T(8,128)(2,1)S(1)} %get-tuple-element.20), channel_id=1, source_target_pairs={{16,0},{0,16},{17,1},{1,17},{18,2},{2,18},{19,3},{3,19},{20,4},{4,... | collective-permute-start | bytes 2113544 | tf_op jit(solution)/shard_map/ppermute | solution.py:139
  225.8 62.1 %copy-start.16 = (bf16[512,4,1,256]{0,3,2,1:T(8,128)(2,1)S(1)}, bf16[512,4,1,256]{0,3,2,1:T(8,128)(2,1)}, u32[]{:S(2)}) copy-start(bf16[512,4,1,256]{0,3,2,1:T(8,128)(2,1)} %get-tuple-element.24) | copy-start | bytes 3145732
  298.3 27.5 %copy-start.25 = (bf16[512,1376]{0,1:T(8,128)(2,1)}, bf16[512,1376]{0,1:T(8,128)(2,1)S(1)}, u32[]{:S(2)}) copy-start(bf16[512,1376]{0,1:T(8,128)(2,1)S(1)} %fusion.10) | copy-start | bytes 4227076
  299.4 11.7 %copy-start.9 = (bf16[512,1376]{0,1:T(8,128)(2,1)S(1)}, bf16[512,1376]{0,1:T(8,128)(2,1)}, u32[]{:S(2)}) copy-start(bf16[512,1376]{0,1:T(8,128)(2,1)} %copy-done.8) | copy-start | bytes 4227076
  299.4 4.3 %collective-permute-start.26 = (bf16[512,256]{0,1:T(8,128)(2,1)S(1)}, bf16[512,256]{0,1:T(8,128)(2,1)S(1)}, u32[]{:S(2)}, u32[]{:S(2)}) collective-permute-start(bf16[512,256]{0,1:T(8,128)(2,1)S(1)} %bitcast.94), channel_id=1, source_target_pairs={{1,0},{0,1},{3,2},{2,3},{5,4},{4,5},{7,6},{6,7},{9,8},{8,9},{11,10... | collective-permute-start | bytes 786440 | tf_op jit(solution)/shard_map/ppermute | solution.py:38
  299.9 11.2 %collective-permute-start.21 = (bf16[128,1376]{0,1:T(8,128)(2,1)S(1)}, bf16[128,1376]{0,1:T(8,128)(2,1)S(1)}, u32[]{:S(2)}, u32[]{:S(2)}) collective-permute-start(bf16[128,1376]{0,1:T(8,128)(2,1)S(1)} %get-tuple-element.27), channel_id=1, source_target_pairs={{16,0},{0,16},{17,1},{1,17},{18,2},{2,18},{19,3},{3,19},{20,4},{4,... | collective-permute-start | bytes 1056776 | tf_op jit(solution)/shard_map/ppermute | solution.py:139
  301.7 16.9 %collective-permute-start.22 = (bf16[128,1376]{0,1:T(8,128)(2,1)S(1)}, bf16[128,1376]{0,1:T(8,128)(2,1)S(1)}, u32[]{:S(2)}, u32[]{:S(2)}) collective-permute-start(bf16[128,1376]{0,1:T(8,128)(2,1)S(1)} %get-tuple-element.25), channel_id=1, source_target_pairs={{16,0},{0,16},{17,1},{1,17},{18,2},{2,18},{19,3},{3,19},{20,4},{4,... | collective-permute-start | bytes 1056776 | tf_op jit(solution)/shard_map/ppermute | solution.py:139
  302.0 23.7 %collective-permute-start.23 = (bf16[128,1376]{0,1:T(8,128)(2,1)S(1)}, bf16[128,1376]{0,1:T(8,128)(2,1)S(1)}, u32[]{:S(2)}, u32[]{:S(2)}) collective-permute-start(bf16[128,1376]{0,1:T(8,128)(2,1)S(1)} %get-tuple-element.26), channel_id=1, source_target_pairs={{16,0},{0,16},{17,1},{1,17},{18,2},{2,18},{19,3},{3,19},{20,4},{4,... | collective-permute-start | bytes 1056776 | tf_op jit(solution)/shard_map/ppermute | solution.py:139
  304.5 56.9 %collective-permute-start.27 = (bf16[512,128]{0,1:T(8,128)(2,1)}, bf16[512,128]{0,1:T(8,128)(2,1)S(1)}, u32[]{:S(2)}, u32[]{:S(2)}) collective-permute-start(bf16[512,128]{0,1:T(8,128)(2,1)} %dynamic-slice_convert_fusion.2), channel_id=1, source_target_pairs={{2,0},{3,1},{0,2},{1,3},{6,4},{7,5},{4,6},{5,7},{10,8},{11,9},{8,1... | collective-permute-start | bytes 393224 | tf_op jit(solution)/shard_map/ppermute | solution.py:38
  327.6 5.8 %collective-permute-start.24 = (bf16[512,256]{0,1:T(8,128)(2,1)}, bf16[512,256]{0,1:T(8,128)(2,1)}, u32[]{:S(2)}, u32[]{:S(2)}) collective-permute-start(bf16[512,256]{0,1:T(8,128)(2,1)} %bitcast.18), channel_id=1, source_target_pairs={{1,0},{0,1},{3,2},{2,3},{5,4},{4,5},{7,6},{6,7},{9,8},{8,9},{11,10... | collective-permute-start | bytes 786440 | tf_op jit(solution)/shard_map/ppermute | solution.py:38
  330.5 13.7 %copy-start.11 = (bf16[512,1376]{0,1:T(8,128)(2,1)S(1)}, bf16[512,1376]{0,1:T(8,128)(2,1)}, u32[]{:S(2)}) copy-start(bf16[512,1376]{0,1:T(8,128)(2,1)} %copy-done.10) | copy-start | bytes 4227076
  330.6 26.2 %copy-start.26 = (bf16[512,1376]{0,1:T(8,128)(2,1)S(1)}, bf16[512,1376]{0,1:T(8,128)(2,1)}, u32[]{:S(2)}) copy-start(bf16[512,1376]{0,1:T(8,128)(2,1)} %copy-done.25) | copy-start | bytes 4227076
  330.6 27.4 %collective-permute-start.33 = (bf16[512,256]{0,1:T(8,128)(2,1)S(1)}, bf16[512,256]{0,1:T(8,128)(2,1)S(1)}, u32[]{:S(2)}, u32[]{:S(2)}) collective-permute-start(bf16[512,256]{0,1:T(8,128)(2,1)S(1)} %bitcast.93), channel_id=1, source_target_pairs={{1,0},{0,1},{3,2},{2,3},{5,4},{4,5},{7,6},{6,7},{9,8},{8,9},{11,10... | collective-permute-start | bytes 786440 | tf_op jit(solution)/shard_map/ppermute | solution.py:38
  331.4 11.2 %collective-permute-start.28 = (bf16[128,1376]{0,1:T(8,128)(2,1)S(1)}, bf16[128,1376]{0,1:T(8,128)(2,1)S(1)}, u32[]{:S(2)}, u32[]{:S(2)}) collective-permute-start(bf16[128,1376]{0,1:T(8,128)(2,1)S(1)} %get-tuple-element.33), channel_id=1, source_target_pairs={{16,0},{0,16},{17,1},{1,17},{18,2},{2,18},{19,3},{3,19},{20,4},{4,... | collective-permute-start | bytes 1056776 | tf_op jit(solution)/shard_map/ppermute | solution.py:139
  333.2 16.9 %collective-permute-start.29 = (bf16[128,1376]{0,1:T(8,128)(2,1)S(1)}, bf16[128,1376]{0,1:T(8,128)(2,1)S(1)}, u32[]{:S(2)}, u32[]{:S(2)}) collective-permute-start(bf16[128,1376]{0,1:T(8,128)(2,1)S(1)} %get-tuple-element.32), channel_id=1, source_target_pairs={{16,0},{0,16},{17,1},{1,17},{18,2},{2,18},{19,3},{3,19},{20,4},{4,... | collective-permute-start | bytes 1056776 | tf_op jit(solution)/shard_map/ppermute | solution.py:139
  333.5 23.2 %collective-permute-start.30 = (bf16[128,1376]{0,1:T(8,128)(2,1)S(1)}, bf16[128,1376]{0,1:T(8,128)(2,1)S(1)}, u32[]{:S(2)}, u32[]{:S(2)}) collective-permute-start(bf16[128,1376]{0,1:T(8,128)(2,1)S(1)} %get-tuple-element.31), channel_id=1, source_target_pairs={{16,0},{0,16},{17,1},{1,17},{18,2},{2,18},{19,3},{3,19},{20,4},{4,... | collective-permute-start | bytes 1056776 | tf_op jit(solution)/shard_map/ppermute | solution.py:139
  342.5 18.9 %collective-permute-start.25 = (bf16[512,128]{0,1:T(8,128)(2,1)S(1)}, bf16[512,128]{0,1:T(8,128)(2,1)S(1)}, u32[]{:S(2)}, u32[]{:S(2)}) collective-permute-start(bf16[512,128]{0,1:T(8,128)(2,1)S(1)} %dynamic-slice_convert_fusion.3), channel_id=1, source_target_pairs={{2,0},{3,1},{0,2},{1,3},{6,4},{7,5},{4,6},{5,7},{10,8},{11,9},{8,1... | collective-permute-start | bytes 393224 | tf_op jit(solution)/shard_map/ppermute | solution.py:38
  357.9 2.0 collective-permute-start.31
  358.1 6.4 %collective-permute-start.34 = (bf16[512,128]{0,1:T(8,128)(2,1)S(1)}, bf16[512,128]{0,1:T(8,128)(2,1)S(1)}, u32[]{:S(2)}, u32[]{:S(2)}) collective-permute-start(bf16[512,128]{0,1:T(8,128)(2,1)S(1)} %dynamic-slice_convert_fusion), channel_id=1, source_target_pairs={{2,0},{3,1},{0,2},{1,3},{6,4},{7,5},{4,6},{5,7},{10,8},{11,9},{8,1... | collective-permute-start | bytes 393224 | tf_op jit(solution)/shard_map/ppermute | solution.py:38
  360.0 6.8 %collective-permute-start.32 = (bf16[512,128]{0,1:T(8,128)(2,1)S(1)}, bf16[512,128]{0,1:T(8,128)(2,1)S(1)}, u32[]{:S(2)}, u32[]{:S(2)}) collective-permute-start(bf16[512,128]{0,1:T(8,128)(2,1)S(1)} %dynamic-slice_convert_fusion.1), channel_id=1, source_target_pairs={{2,0},{3,1},{0,2},{1,3},{6,4},{7,5},{4,6},{5,7},{10,8},{11,9},{8,1... | collective-permute-start | bytes 393224 | tf_op jit(solution)/shard_map/ppermute | solution.py:38
  (18 other events, 64.3 us)
Sparse Core Ops, SparseCore 0:
  45.1 100.6 all-gather.4
  147.3 57.9 all-gather.6
  206.9 33.2 all-gather.8
  241.6 33.2 all-gather.10
